TPU v7x, 32 devices: a whole 2x2x4 slice. The times are simulated.
32 devices in a mesh: fs: 8 (over z, y), tp: 4 (over x, core).
Axes of the slice: x: 2, y: 2, z: 4, core: 2. Of those that a mesh axis runs over, the one named last changes fastest.
Arguments:
- x_late: bfloat16 [6144, 2048], P(('fs', 'tp')), may hold values from -6 to 6
- x_early: bfloat16 [6144, 2048], P(('fs', 'tp')), may hold values from -6 to 6
- w_gate: bfloat16 [2048, 5632], P('fs', 'tp'), may hold values from -0.125 to 0.125
- w_value: bfloat16 [2048, 5632], P('fs', 'tp'), may hold values from -0.125 to 0.125
- conv_taps: float32 [3, 5632], P(None, 'tp'), may hold values from -3 to 3
- grad_hidden: bfloat16 [6144, 5632], P('fs', 'tp'), may hold values from -6 to 6
- sum_gate: float32 [2048, 5632], P('fs', 'tp'), may hold values from -6 to 6
- sum_value: float32 [2048, 5632], P('fs', 'tp'), may hold values from -6 to 6
- sum_taps: float32 [3, 5632], P(None, 'tp'), may hold values from -6 to 6
Outputs:
- hidden_late: bfloat16 [6144, 5632], P('fs', 'tp')
- grad_early: bfloat16 [6144, 2048], P(('fs', 'tp'))
- new_sum_gate: float32 [2048, 5632], P('fs', 'tp')
- new_sum_value: float32 [2048, 5632], P('fs', 'tp')
- new_sum_taps: float32 [3, 5632], P(None, 'tp')
All inputs are finite; a program needn't handle non-finite values.
Results may differ from a plain program's by a relative error of at most 0.015.
Values may be sent and summed in bfloat16 or wider, within the bound.
A program may use at most 128 MiB of HBM per device.

v0:
```python
import math
import jax
import jax.numpy as jnp
from jax import lax
from jax.sharding import PartitionSpec as P

root_half = 0.7071067811865476
density_norm = 0.3989422804014327


def causal_mix(gate_rows, taps):
    width = taps.shape[0]
    length = gate_rows.shape[0]
    padded = jnp.pad(gate_rows.astype(jnp.float32), ((width - 1, 0), (0, 0)))
    mixed_pre = jnp.zeros((length, gate_rows.shape[1]), jnp.float32)
    for j in range(width):
        mixed_pre = mixed_pre + padded[j : j + length] * taps[j]
    return (mixed_pre, padded)


def gelu_slope(mixed_pre):
    return (
        0.5 * (1.0 + lax.erf(mixed_pre * root_half))
        + mixed_pre * jnp.exp(-0.5 * mixed_pre * mixed_pre) * density_norm
    )


def back_mix(slope_rows, taps, padded):
    width = taps.shape[0]
    length = slope_rows.shape[0]
    grown = jnp.pad(slope_rows, ((0, width - 1), (0, 0)))
    d_gate = jnp.zeros(slope_rows.shape, jnp.float32)
    for j in range(width):
        d_gate = d_gate + grown[width - 1 - j : width - 1 - j + length] * taps[j]
    tap_terms = jnp.stack(
        [jnp.sum(slope_rows * padded[j : j + length], axis=0) for j in range(width)]
    )
    return (d_gate, tap_terms)


def shards(x_late, x_early, w_gate, w_value, conv_taps, grad_hidden, sum_gate, sum_value, sum_taps):
    columns = w_gate.shape[1]
    factor = 1.0 / math.sqrt(x_late.shape[0] * lax.axis_size("fs") * lax.axis_size("tp"))
    gate_full, value_full = (
        lax.all_gather(w_gate, "fs", axis=0, tiled=True),
        lax.all_gather(w_value, "fs", axis=0, tiled=True),
    )
    block_rows = lax.all_gather(x_late, "tp", axis=0, tiled=True)
    gate_part = jnp.dot(block_rows, gate_full, preferred_element_type=jnp.float32).astype(
        jnp.bfloat16
    )
    value_part = jnp.dot(block_rows, value_full, preferred_element_type=jnp.float32).astype(
        jnp.bfloat16
    )
    projected = jnp.concatenate([gate_part, value_part], axis=1)
    gate_rows = projected[:, :columns]
    value_rows = projected[:, columns:]
    mixed_pre, padded = causal_mix(gate_rows, conv_taps)
    hidden = (jax.nn.gelu(mixed_pre, approximate=False) * value_rows.astype(jnp.float32)).astype(
        jnp.bfloat16
    )
    gathered = lax.all_gather(x_early, "tp", axis=0, tiled=True)
    gate_rows = jnp.dot(gathered, gate_full, preferred_element_type=jnp.float32).astype(
        jnp.bfloat16
    )
    value_rows = jnp.dot(gathered, value_full, preferred_element_type=jnp.float32).astype(
        jnp.bfloat16
    )
    mixed_pre, padded = causal_mix(gate_rows, conv_taps)
    upstream = grad_hidden.astype(jnp.float32)
    slope_rows = upstream * value_rows.astype(jnp.float32) * gelu_slope(mixed_pre)
    d_gate_f, tap_terms = back_mix(slope_rows, conv_taps, padded)
    d_gate = d_gate_f.astype(jnp.bfloat16)
    d_value = (upstream * jax.nn.gelu(mixed_pre, approximate=False)).astype(jnp.bfloat16)
    contract = (((1,), (1,)), ((), ()))
    grad_early = lax.psum_scatter(
        (
            lax.dot_general(d_gate, gate_full, contract, preferred_element_type=jnp.float32)
            + lax.dot_general(d_value, value_full, contract, preferred_element_type=jnp.float32)
        ).astype(jnp.bfloat16),
        "tp",
        scatter_dimension=0,
        tiled=True,
    )
    both_grads = jnp.concatenate([d_gate, d_value], axis=1)
    product = lax.dot_general(
        gathered, both_grads, (((0,), (0,)), ((), ())), preferred_element_type=jnp.float32
    )
    totals = lax.psum_scatter(
        (factor * product).astype(jnp.bfloat16), "fs", scatter_dimension=0, tiled=True
    ).astype(jnp.float32)
    gate_total = totals[:, :columns]
    value_total = totals[:, columns:]
    tap_total = lax.psum(factor * tap_terms, "fs")
    return (
        hidden,
        grad_early,
        sum_gate + gate_total,
        sum_value + value_total,
        sum_taps + tap_total,
    )


def solution(mesh):
    placed = (
        P(("fs", "tp"), None),
        P(("fs", "tp"), None),
        P("fs", "tp"),
        P("fs", "tp"),
        P(None, "tp"),
        P("fs", "tp"),
        P("fs", "tp"),
        P("fs", "tp"),
        P(None, "tp"),
    )
    return jax.shard_map(
        shards,
        mesh=mesh,
        in_specs=placed,
        out_specs=(
            P("fs", "tp"),
            P(("fs", "tp"), None),
            P("fs", "tp"),
            P("fs", "tp"),
            P(None, "tp"),
        ),
        check_vma=False,
    )
```

profile of v0, /device:TPU:0, one launch (start us, length us, event | category | flops | bytes accessed | tf_op | source)
XLA Modules:
  0.0 500.2 jit_solution(172343307863899647)
XLA Ops:
  7.2 0.7 all-gather.11.cloned.1.call-update
  7.9 0.0 all-gather.7.cloned.1.call-start
  7.9 0.7 all-gather.7.cloned.1.call-update
  8.7 0.7 all-gather.9.cloned.1.call-update
  9.4 0.5 all-gather.5.cloned.1.call-update
  10.0 0.0 reduce-scatter.5.cloned.1.call-start
  10.0 0.9 slice_reduce_fusion.2
  10.9 29.9 %all-gather.11.cloned.1.call-done = bf16[768,2048]{1,0:T(8,128)(2,1)} async-done(((bf16[192,2048]{1,0:T(8,128)(2,1)}), bf16[768,2048]{1,0:T(8,128)(2,1)}) %all-gather.11.cloned.1.call-update) | async-done | bytes 3145744 | tf_op jit(solution)/shard_map/all_gather | solution.py:62
  40.8 94.5 %all-gather.7.cloned.1.call-done = bf16[2048,1408]{1,0:T(8,128)(2,1)} async-done(((bf16[256,1408]{1,0:T(8,128)(2,1)}), bf16[2048,1408]{1,0:T(8,128)(2,1)}) %all-gather.7.cloned.1.call-update) | async-done | bytes 5767184 | tf_op jit(solution)/shard_map/all_gather | solution.py:45
  135.3 8.4 %fusion.30 = f32[768,1408]{1,0:T(8,128)S(1)} fusion(bf16[768,2048]{1,0:T(8,128)(2,1)} %all-gather.11.cloned.1.call-done, bf16[2048,1408]{1,0:T(8,128)(2,1)} %all-gather.7.cloned.1.call-done), kind=kOutput, calls=%fused_computation.62 | convolution fusion | flops 4431347712 | bytes 13238272 | tf_op jit(solution)/shard_map/dot_general | solution.py:63
  143.8 2.0 copy-done
  145.7 11.8 %fusion.2 = (bf16[768,1408]{1,0:T(8,128)(2,1)}, f32[768,1408]{1,0:T(8,128)}) fusion(bf16[768,1408]{1,0:T(8,128)(2,1)S(1)} %copy-done.2, f32[768,1408]{1,0:T(8,128)S(1)} %fusion.30, f32[1408]{0:T(1024)S(1)} %get-tuple-element.14, f32[1408]{0:T(1024)S(1)} %get-tuple-element.15, f32[1408]{0:T(1024)S(1)} %get-tuple-element.13), kind=kLoop, calls=%fused_computation.9 | loop fusion | flops 77856768 | bytes 12993024 | tf_op jit(solution)/shard_map/convert_element_type | solution.py:74
  157.6 70.5 %all-gather.9.cloned.1.call-done = bf16[2048,1408]{1,0:T(8,128)(2,1)} async-done(((bf16[256,1408]{1,0:T(8,128)(2,1)}), bf16[2048,1408]{1,0:T(8,128)(2,1)}) %all-gather.9.cloned.1.call-update) | async-done | bytes 5767184 | tf_op jit(solution)/shard_map/all_gather | solution.py:46
  228.0 9.8 %fusion.1 = f32[768,1408]{1,0:T(8,128)S(1)} fusion(bf16[768,1408]{1,0:T(8,128)(2,1)S(1)} %copy-done.2, f32[768,1408]{1,0:T(8,128)} %get-tuple-element.17, bf16[768,2048]{1,0:T(8,128)(2,1)} %all-gather.11.cloned.1.call-done, bf16[2048,1408]{1,0:T(8,128)(2,1)} %all-gather.9.cloned.1.call-done), kind=kOutput, calls=%fused_computation.8 | convolution fusion | flops 4443242496 | bytes 19726336 | tf_op jit(solution)/shard_map/dot_general | solution.py:66
  237.9 3.0 multiply_reduce_fusion.2
  240.9 1.3 copy-done.4
  242.3 12.1 %fusion = bf16[2048,2816]{0,1:T(8,128)(2,1)} fusion(bf16[768,2048]{1,0:T(8,128)(2,1)S(1)} %copy-done.7, bf16[768,1408]{1,0:T(8,128)(2,1)S(1)} %copy-done.3, bf16[768,1408]{1,0:T(8,128)(2,1)S(1)} %get-tuple-element.18), kind=kOutput, calls=%fused_computation.1 | convolution fusion | flops 8878555136 | bytes 19005440 | tf_op jit(solution)/shard_map/dot_general | solution.py:86
  254.4 0.0 reduce-scatter.3.cloned.1.call-start
  254.5 7.8 %fusion.33 = f32[768,2048]{1,0:T(8,128)S(1)} fusion(bf16[768,1408]{1,0:T(8,128)(2,1)} %copy-done.4, bf16[2048,1408]{1,0:T(8,128)(2,1)} %all-gather.7.cloned.1.call-done), kind=kOutput, calls=%fused_computation.74 | convolution fusion | flops 4429185024 | bytes 14221312 | tf_op jit(solution)/shard_map/dot_general | solution.py:78
  262.3 9.2 %add_convert_fusion = bf16[768,2048]{1,0:T(8,128)(2,1)} fusion(f32[768,2048]{1,0:T(8,128)S(1)} %fusion.33, bf16[768,1408]{1,0:T(8,128)(2,1)S(1)} %copy-done.3, bf16[2048,1408]{1,0:T(8,128)(2,1)} %all-gather.9.cloned.1.call-done), kind=kOutput, calls=%fused_computation.5 | convolution fusion | flops 4432330752 | bytes 17367040 | tf_op jit(solution)/shard_map/dot_general | solution.py:79
  271.5 1.8 copy.14
  273.3 1.8 copy.15
  275.2 36.6 %psum.7 = f32[3,1408]{1,0:T(4,128)S(1)} all-reduce(f32[3,1408]{1,0:T(4,128)S(1)} %maximum_multiply_fusion), channel_id=1, replica_groups=mesh['fs'=8,'tp'=4] {'fs'}, use_global_device_ids=true, to_apply=%region_5.6 | all-reduce | flops 4224 | bytes 33792 | tf_op jit(solution)/shard_map/psum | solution.py:94
  311.8 0.6 add.59
  312.4 9.0 %fusion.31 = f32[768,1408]{1,0:T(8,128)S(1)} fusion(bf16[768,2048]{1,0:T(8,128)(2,1)} %all-gather.5.cloned.1.call-done, bf16[2048,1408]{1,0:T(8,128)(2,1)} %all-gather.7.cloned.1.call-done), kind=kOutput, calls=%fused_computation.66 | convolution fusion | flops 4431347712 | bytes 13238272 | tf_op jit(solution)/shard_map/dot_general | solution.py:49
  321.4 19.9 %fusion.6 = bf16[768,1408]{1,0:T(8,128)(2,1)} fusion(f32[768,1408]{1,0:T(8,128)S(1)} %fusion.31, bf16[768,2048]{1,0:T(8,128)(2,1)S(1)} %copy-done.6, bf16[2048,1408]{1,0:T(8,128)(2,1)} %all-gather.9.cloned.1.call-done, f32[1408]{0:T(1024)S(1)} %get-tuple-element.14, f32[1408]{0:T(1024)S(1)} %get-tuple-element.15, f32[1408]{0:T(1024)S(1)} %get-tuple-element.13), kind=kOutput, calls=%fused_computation.13 | convolution fusion | flops 4508123136 | bytes 15417856 | tf_op jit(solution)/shard_map/dot_general | solution.py:52
  341.3 112.0 %reduce-scatter.5.cloned.1.call-done = bf16[256,2816]{0,1:T(8,128)(2,1)} async-done(((bf16[2048,2816]{0,1:T(8,128)(2,1)}), bf16[256,2816]{0,1:T(8,128)(2,1)}) %reduce-scatter.5.cloned.1.call-update) | async-done | bytes 1441808 | tf_op jit(solution)/shard_map/reduce_scatter | solution.py:89
  453.4 1.6 convert_element_type.68
  454.9 1.9 slice_add_fusion
  456.9 2.9 copy.16
  459.8 3.2 copy.17
  463.0 30.4 %reduce-scatter.3.cloned.1.call-done = bf16[192,2048]{1,0:T(8,128)(2,1)} async-done(((bf16[768,2048]{1,0:T(8,128)(2,1)}), bf16[192,2048]{1,0:T(8,128)(2,1)}) %reduce-scatter.3.cloned.1.call-update) | async-done | bytes 786448 | tf_op jit(solution)/shard_map/reduce_scatter | solution.py:76
  (24 shorter events, 0.2 us)
Async XLA Ops:
  7.2 33.6 %all-gather.11.cloned.1.call-start = ((), (), s32[]{:S(2)}) async-start(), calls=%async_computation.5 | async-start | bytes 3932160 | tf_op jit(solution)/shard_map/all_gather | solution.py:62
  7.9 127.4 %all-gather.7.cloned.1.call-start = ((), (), s32[]{:S(2)}) async-start(), calls=%async_computation.3 | async-start | bytes 6488064 | tf_op jit(solution)/shard_map/all_gather | solution.py:45
  8.6 219.4 %all-gather.9.cloned.1.call-start = ((), (), s32[]{:S(2)}) async-start(), calls=%async_computation.4 | async-start | bytes 6488064 | tf_op jit(solution)/shard_map/all_gather | solution.py:46
  9.4 303.0 %all-gather.5.cloned.1.call-start = ((), (), s32[]{:S(2)}) async-start(), calls=%async_computation.2 | async-start | bytes 3932160 | tf_op jit(solution)/shard_map/all_gather | solution.py:48
  10.0 443.4 %reduce-scatter.5.cloned.1.call-start = ((), (), s32[]{:S(2)}) async-start(), calls=%async_computation.7 | async-start | bytes 12976128 | tf_op jit(solution)/shard_map/reduce_scatter | solution.py:89
  10.9 134.8 %copy-start.2 = (bf16[768,1408]{1,0:T(8,128)(2,1)S(1)}, bf16[768,1408]{1,0:T(8,128)(2,1)}, u32[]{:S(2)}) copy-start(bf16[768,1408]{1,0:T(8,128)(2,1)} %param.14) | copy-start | bytes 6488068
  143.7 2.0 copy-start
  228.0 9.9 %copy-start.1 = (f32[768,1408]{1,0:T(8,128)S(1)}, f32[768,1408]{1,0:T(8,128)}, u32[]{:S(2)}) copy-start(f32[768,1408]{1,0:T(8,128)} %copy-done) | copy-start | bytes 12976132
  237.9 4.4 copy-start.3
  237.9 4.4 copy-start.7
  240.9 1.3 copy-start.4
  254.4 238.9 %reduce-scatter.3.cloned.1.call-start = ((), (), s32[]{:S(2)}) async-start(), calls=%async_computation.6 | async-start | bytes 3932160 | tf_op jit(solution)/shard_map/reduce_scatter | solution.py:76
  271.5 40.3 %copy-start.5 = (f32[3,1408]{1,0:T(4,128)S(1)}, f32[3,1408]{1,0:T(4,128)}, u32[]{:S(2)}) copy-start(f32[3,1408]{1,0:T(4,128)} %param.17) | copy-start | bytes 50692
  312.4 9.0 %copy-start.6 = (bf16[768,2048]{1,0:T(8,128)(2,1)S(1)}, bf16[768,2048]{1,0:T(8,128)(2,1)}, u32[]{:S(2)}) copy-start(bf16[768,2048]{1,0:T(8,128)(2,1)} %all-gather.5.cloned.1.call-done) | copy-start | bytes 9437188
Sparse Core Ops, SparseCore 0:
  9.5 31.2 all-gather.10
  43.0 92.3 all-gather.6
  137.5 90.4 all-gather.8
  229.4 26.6 all-gather.4
  259.6 193.6 reduce-scatter.4
  456.3 37.0 reduce-scatter.2
where the time goes:
time: 501 us; the launch traced here: 500 us
  waiting for transfers between devices  340 us (68%)
  matrix products  76.3 us (15%)
  blocking collectives  36.6 us (7%)
  other arithmetic  19 us (4%)
  between operations  14.3 us (3%)
  local copies, waits for them, and re-layouts  14 us (3%)
    reduce_scatter x1, waiting for transfers between devices, shards(): lax.psum_scatter((factor * product).astype(jnp.bfloat16), 'fs', scatter_d...  112 us
    all_gather x1, waiting for transfers between devices, shards(): lax.all_gather(w_gate, 'fs', axis=0, tiled=True)  94.5 us
    all_gather x1, waiting for transfers between devices, shards(): lax.all_gather(w_value, 'fs', axis=0, tiled=True)  70.5 us
    psum x1, blocking collectives, shards(): tap_total = lax.psum(factor * tap_terms, 'fs')  36.6 us
    reduce_scatter x1, waiting for transfers between devices, shards(): lax.psum_scatter((lax.dot_general(d_gate, gate_full, contract, preferred_...  30.4 us
    all_gather x1, waiting for transfers between devices, shards(): gathered = lax.all_gather(x_early, 'tp', axis=0, tiled=True)  29.9 us
    dot_general x1, matrix products, shards(): jnp.dot(block_rows, value_full, preferred_element_type=jnp.float32)  19.9 us
    unnamed x20, local copies, waits for them, and re-layouts  13.1 us
  transfers between devices with their start and end apart: 6, of which 5 were waited for; matrix products, arithmetic and copies ran while one was open for 21% of the time, Pallas kernels for 0%

commit v1 on v0

--- a/solution.py
+++ b/solution.py
@@ -59,7 +59,13 @@
     hidden = (jax.nn.gelu(mixed_pre, approximate=False) * value_rows.astype(jnp.float32)).astype(
         jnp.bfloat16
     )
-    gathered = lax.all_gather(x_early, "tp", axis=0, tiled=True)
+    count = lax.axis_size("tp")
+    held, pieces = (x_early, [x_early])
+    for _ in range(count - 1):
+        held = lax.ppermute(held, "tp", [(i, (i + 1) % count) for i in range(count)])
+        pieces.insert(0, held)
+    line = jnp.concatenate(pieces, axis=0)
+    gathered = jnp.roll(line, (lax.axis_index("tp") + 1) * x_early.shape[0], axis=0)
     gate_rows = jnp.dot(gathered, gate_full, preferred_element_type=jnp.float32).astype(
         jnp.bfloat16
     )

time: 501 us -> 470 us (0.938)
  waiting for transfers between devices: 340 us -> 308 us
    all_gather x1, waiting for transfers between devices: 94.5 us -> 53.8 us  [shards(): lax.all_gather(w_gate, 'fs', axis=0, tiled=True)]
    ppermute x0 -> x3, waiting for transfers between devices: none -> 33.6 us  [shards(): lax.ppermute(held, 'tp', [(i, (i + 1) % count) for i in range(count)])]
    all_gather x1 -> x0, waiting for transfers between devices: 29.9 us -> none  [shards(): gathered = lax.all_gather(x_early, 'tp', axis=0, tiled=True)]
    reduce_scatter x1, waiting for transfers between devices: 30.4 us -> 36.3 us  [shards(): lax.psum_scatter((lax.dot_general(d_gate, gate_full, contract, preferred_...]
    unnamed x20 -> x27, local copies, waits for them, and re-layouts: 13.1 us -> 10.1 us
  transfers between devices with their start and end apart: 6 -> 8, of which waited for: 5 -> 7; matrix products, arithmetic and copies ran while one was open for 21% -> 23% of each run, Pallas kernels for 0% -> 0%
where the time goes in v1:
time: 470 us; the launch traced here: 469 us
  waiting for transfers between devices  308 us (66%)
  matrix products  80.4 us (17%)
  blocking collectives  35.6 us (8%)
  other arithmetic  19 us (4%)
  between operations  14 us (3%)
  local copies, waits for them, and re-layouts  11.9 us (3%)
    reduce_scatter x1, waiting for transfers between devices, shards(): lax.psum_scatter((factor * product).astype(jnp.bfloat16), 'fs', scatter_d...  112 us
    all_gather x1, waiting for transfers between devices, shards(): lax.all_gather(w_value, 'fs', axis=0, tiled=True)  70.4 us
    all_gather x1, waiting for transfers between devices, shards(): lax.all_gather(w_gate, 'fs', axis=0, tiled=True)  53.8 us
    reduce_scatter x1, waiting for transfers between devices, shards(): lax.psum_scatter((lax.dot_general(d_gate, gate_full, contract, preferred_...  36.3 us
    psum x1, blocking collectives, shards(): tap_total = lax.psum(factor * tap_terms, 'fs')  35.6 us
    ppermute x3, waiting for transfers between devices, shards(): lax.ppermute(held, 'tp', [(i, (i + 1) % count) for i in range(count)])  33.6 us
    dot_general x1, matrix products, shards(): jnp.dot(block_rows, value_full, preferred_element_type=jnp.float32)  19.9 us
    dot_general x1, matrix products, shards(): lax.dot_general(gathered, both_grads, (((0,), (0,)), ((), ())), preferred...  15.1 us
  transfers between devices with their start and end apart: 8, of which 7 were waited for; matrix products, arithmetic and copies ran while one was open for 23% of the time, Pallas kernels for 0%

profile of v1, /device:TPU:0, one launch (start us, length us, event | category | flops | bytes accessed | tf_op | source)
XLA Modules:
  0.0 469.3 jit_solution(16289531635578527128)
XLA Ops:
  7.2 0.7 all-gather.6.cloned.1.call-update
  8.0 0.7 all-gather.8.cloned.1.call-update
  9.2 11.8 %collective-permute-done = bf16[192,2048]{1,0:T(8,128)(2,1)S(1)} collective-permute-done((bf16[192,2048]{1,0:T(8,128)(2,1)}, bf16[192,2048]{1,0:T(8,128)(2,1)S(1)}, u32[]{:S(2)}, u32[]{:S(2)}) %collective-permute-start) | collective-permute-done | bytes 786464 | tf_op jit(solution)/shard_map/ppermute | solution.py:65
  21.1 11.4 %collective-permute-done.1 = bf16[192,2048]{1,0:T(8,128)(2,1)S(1)} collective-permute-done((bf16[192,2048]{1,0:T(8,128)(2,1)S(1)}, bf16[192,2048]{1,0:T(8,128)(2,1)S(1)}, u32[]{:S(2)}, u32[]{:S(2)}) %collective-permute-start.1) | collective-permute-done | bytes 786464 | tf_op jit(solution)/shard_map/ppermute | solution.py:65
  32.6 0.9 slice_reduce_fusion.2
  33.5 10.4 %collective-permute-done.2 = bf16[192,2048]{1,0:T(8,128)(2,1)S(1)} collective-permute-done((bf16[192,2048]{1,0:T(8,128)(2,1)S(1)}, bf16[192,2048]{1,0:T(8,128)(2,1)S(1)}, u32[]{:S(2)}, u32[]{:S(2)}) %collective-permute-start.2) | collective-permute-done | bytes 786464 | tf_op jit(solution)/shard_map/ppermute | solution.py:65
  43.9 0.9 constant_dynamic-update-slice_fusion.7
  44.8 1.0 constant_dynamic-update-slice_fusion.6
  45.8 1.0 constant_dynamic-update-slice_fusion.5
  46.7 1.0 constant_dynamic-update-slice_fusion.4
  47.7 0.9 constant_dynamic-update-slice_fusion.3
  48.7 0.9 constant_dynamic-update-slice_fusion.2
  49.6 0.9 constant_dynamic-update-slice_fusion.1
  50.5 1.0 constant_dynamic-update-slice_fusion
  51.5 53.8 %all-gather.6.cloned.1.call-done = bf16[2048,1408]{1,0:T(8,128)(2,1)} async-done(((bf16[256,1408]{1,0:T(8,128)(2,1)}), bf16[2048,1408]{1,0:T(8,128)(2,1)}) %all-gather.6.cloned.1.call-update) | async-done | bytes 5767184 | tf_op jit(solution)/shard_map/all_gather | solution.py:45
  105.2 8.4 %fusion.29 = f32[768,1408]{1,0:T(8,128)S(1)} fusion(bf16[2048,1408]{1,0:T(8,128)(2,1)} %all-gather.6.cloned.1.call-done, bf16[1536,2048]{1,0:T(8,128)(2,1)} %constant_dynamic-update-slice_fusion, s32[]{:T(128)S(6)} %select_n.14), kind=kOutput, calls=%fused_computation.61 | convolution fusion | flops 4431347712 | bytes 13238276 | tf_op jit(solution)/shard_map/dot_general | solution.py:69
  113.7 2.0 copy-done
  115.7 11.8 %fusion.1 = (bf16[768,1408]{1,0:T(8,128)(2,1)}, f32[768,1408]{1,0:T(8,128)}) fusion(bf16[768,1408]{1,0:T(8,128)(2,1)S(1)} %copy-done.3, f32[768,1408]{1,0:T(8,128)S(1)} %fusion.29, f32[1408]{0:T(1024)S(1)} %get-tuple-element.9, f32[1408]{0:T(1024)S(1)} %get-tuple-element.10, f32[1408]{0:T(1024)S(1)} %get-tuple-element.8), kind=kLoop, calls=%fused_computation.8 | loop fusion | flops 77856768 | bytes 12993024 | tf_op jit(solution)/shard_map/convert_element_type | solution.py:80
  127.5 70.4 %all-gather.8.cloned.1.call-done = bf16[2048,1408]{1,0:T(8,128)(2,1)} async-done(((bf16[256,1408]{1,0:T(8,128)(2,1)}), bf16[2048,1408]{1,0:T(8,128)(2,1)}) %all-gather.8.cloned.1.call-update) | async-done | bytes 5767184 | tf_op jit(solution)/shard_map/all_gather | solution.py:46
  197.9 9.9 %fusion = f32[768,1408]{1,0:T(8,128)S(1)} fusion(bf16[768,1408]{1,0:T(8,128)(2,1)S(1)} %copy-done.3, f32[768,1408]{1,0:T(8,128)} %get-tuple-element.12, bf16[2048,1408]{1,0:T(8,128)(2,1)} %all-gather.8.cloned.1.call-done, bf16[1536,2048]{1,0:T(8,128)(2,1)} %constant_dynamic-update-slice_fusion, s32[]{:T(128)S(6)} %select_n.14), kind=kOutput, calls=%fused_computation.7 | convolution fusion | flops 4443242496 | bytes 19726340 | tf_op jit(solution)/shard_map/dot_general | solution.py:72
  207.9 3.0 multiply_reduce_fusion.2
  210.9 1.3 copy-done.5
  212.2 15.1 %multiply_convert_fusion = bf16[2048,2816]{1,0:T(8,128)(2,1)} fusion(bf16[768,1408]{1,0:T(8,128)(2,1)S(1)} %copy-done.4, bf16[768,1408]{1,0:T(8,128)(2,1)S(1)} %get-tuple-element.13, bf16[1536,2048]{1,0:T(8,128)(2,1)} %constant_dynamic-update-slice_fusion, s32[]{:T(128)S(6)} %select_n.14), kind=kOutput, calls=%fused_computation | convolution fusion | flops 8878555136 | bytes 19005444 | tf_op jit(solution)/shard_map/dot_general | solution.py:92
  227.4 7.8 %fusion.38 = f32[768,2048]{1,0:T(8,128)S(1)} fusion(bf16[768,1408]{1,0:T(8,128)(2,1)} %copy-done.5, bf16[2048,1408]{1,0:T(8,128)(2,1)} %all-gather.6.cloned.1.call-done), kind=kOutput, calls=%fused_computation.87 | convolution fusion | flops 4429185024 | bytes 14221312 | tf_op jit(solution)/shard_map/dot_general | solution.py:84
  235.2 10.2 %add_convert_fusion = bf16[768,2048]{1,0:T(8,128)(2,1)} fusion(f32[768,2048]{1,0:T(8,128)S(1)} %fusion.38, bf16[768,1408]{1,0:T(8,128)(2,1)S(1)} %copy-done.4, bf16[2048,1408]{1,0:T(8,128)(2,1)} %all-gather.8.cloned.1.call-done), kind=kOutput, calls=%fused_computation.4 | convolution fusion | flops 4432330752 | bytes 17367040 | tf_op jit(solution)/shard_map/dot_general | solution.py:85
  245.5 35.6 %psum.7 = f32[3,1408]{1,0:T(4,128)S(1)} all-reduce(f32[3,1408]{1,0:T(4,128)S(1)} %maximum_multiply_fusion), channel_id=1, replica_groups=mesh['fs'=8,'tp'=4] {'fs'}, use_global_device_ids=true, to_apply=%region_5.6 | all-reduce | flops 4224 | bytes 33792 | tf_op jit(solution)/shard_map/psum | solution.py:100
  281.8 9.0 %fusion.30 = f32[768,1408]{1,0:T(8,128)S(1)} fusion(bf16[768,2048]{1,0:T(8,128)(2,1)} %all-gather.4.cloned.1.call-done, bf16[2048,1408]{1,0:T(8,128)(2,1)} %all-gather.6.cloned.1.call-done), kind=kOutput, calls=%fused_computation.65 | convolution fusion | flops 4431347712 | bytes 13238272 | tf_op jit(solution)/shard_map/dot_general | solution.py:49
  290.8 19.9 %fusion.5 = bf16[768,1408]{1,0:T(8,128)(2,1)} fusion(f32[768,1408]{1,0:T(8,128)S(1)} %fusion.30, bf16[768,2048]{1,0:T(8,128)(2,1)S(1)} %copy-done.9, bf16[2048,1408]{1,0:T(8,128)(2,1)} %all-gather.8.cloned.1.call-done, f32[1408]{0:T(1024)S(1)} %get-tuple-element.9, f32[1408]{0:T(1024)S(1)} %get-tuple-element.10, f32[1408]{0:T(1024)S(1)} %get-tuple-element.8), kind=kOutput, calls=%fused_computation.12 | convolution fusion | flops 4508123136 | bytes 15417856 | tf_op jit(solution)/shard_map/dot_general | solution.py:52
  310.8 112.0 %reduce-scatter.5.cloned.1.call-done = bf16[256,2816]{1,0:T(8,128)(2,1)} async-done(((bf16[2048,2816]{1,0:T(8,128)(2,1)}), bf16[256,2816]{1,0:T(8,128)(2,1)}) %reduce-scatter.5.cloned.1.call-update) | async-done | bytes 1441808 | tf_op jit(solution)/shard_map/reduce_scatter | solution.py:95
  422.7 1.7 convert_element_type.64
  424.5 1.9 slice_add_fusion
  426.4 36.3 %reduce-scatter.3.cloned.1.call-done = bf16[192,2048]{1,0:T(8,128)(2,1)} async-done(((bf16[768,2048]{1,0:T(8,128)(2,1)}), bf16[192,2048]{1,0:T(8,128)(2,1)}) %reduce-scatter.3.cloned.1.call-update) | async-done | bytes 786448 | tf_op jit(solution)/shard_map/reduce_scatter | solution.py:82
  (35 shorter events, 1.6 us)
Async XLA Ops:
  7.2 39.6 %copy-start.2 = (bf16[192,2048]{1,0:T(8,128)(2,1)S(1)}, bf16[192,2048]{1,0:T(8,128)(2,1)}, u32[]{:S(2)}) copy-start(bf16[192,2048]{1,0:T(8,128)(2,1)} %param.10) | copy-start | bytes 2359300
  7.2 98.1 %all-gather.6.cloned.1.call-start = ((), (), s32[]{:S(2)}) async-start(), calls=%async_computation.3 | async-start | bytes 6488064 | tf_op jit(solution)/shard_map/all_gather | solution.py:45
  7.9 190.0 %all-gather.8.cloned.1.call-start = ((), (), s32[]{:S(2)}) async-start(), calls=%async_computation.4 | async-start | bytes 6488064 | tf_op jit(solution)/shard_map/all_gather | solution.py:46
  8.7 273.1 %all-gather.4.cloned.1.call-start = ((), (), s32[]{:S(2)}) async-start(), calls=%async_computation.2 | async-start | bytes 3932160 | tf_op jit(solution)/shard_map/all_gather | solution.py:48
  8.7 12.3 %collective-permute-start = (bf16[192,2048]{1,0:T(8,128)(2,1)}, bf16[192,2048]{1,0:T(8,128)(2,1)S(1)}, u32[]{:S(2)}, u32[]{:S(2)}) collective-permute-start(bf16[192,2048]{1,0:T(8,128)(2,1)} %param.10), channel_id=1, source_target_pairs={{0,1},{1,2},{2,3},{3,0},{4,5},{5,6},{6,7},{7,4},{8,9},{9,10},{10,1... | collective-permute-start | bytes 2359304 | tf_op jit(solution)/shard_map/ppermute | solution.py:65
  21.0 11.4 %collective-permute-start.1 = (bf16[192,2048]{1,0:T(8,128)(2,1)S(1)}, bf16[192,2048]{1,0:T(8,128)(2,1)S(1)}, u32[]{:S(2)}, u32[]{:S(2)}) collective-permute-start(bf16[192,2048]{1,0:T(8,128)(2,1)S(1)} %collective-permute-done), channel_id=1, source_target_pairs={{0,1},{1,2},{2,3},{3,0},{4,5},{5,6},{6,7},{7,4},{8,9},{9,10},{10,1... | collective-permute-start | bytes 2359304 | tf_op jit(solution)/shard_map/ppermute | solution.py:65
  32.5 11.4 %collective-permute-start.2 = (bf16[192,2048]{1,0:T(8,128)(2,1)S(1)}, bf16[192,2048]{1,0:T(8,128)(2,1)S(1)}, u32[]{:S(2)}, u32[]{:S(2)}) collective-permute-start(bf16[192,2048]{1,0:T(8,128)(2,1)S(1)} %collective-permute-done.1), channel_id=1, source_target_pairs={{0,1},{1,2},{2,3},{3,0},{4,5},{5,6},{6,7},{7,4},{8,9},{9,10},{10,1... | collective-permute-start | bytes 2359304 | tf_op jit(solution)/shard_map/ppermute | solution.py:65
  32.5 390.3 %reduce-scatter.5.cloned.1.call-start = ((), (), s32[]{:S(2)}) async-start(), calls=%async_computation.6 | async-start | bytes 12976128 | tf_op jit(solution)/shard_map/reduce_scatter | solution.py:95
  51.5 64.2 %copy-start.3 = (bf16[768,1408]{1,0:T(8,128)(2,1)S(1)}, bf16[768,1408]{1,0:T(8,128)(2,1)}, u32[]{:S(2)}) copy-start(bf16[768,1408]{1,0:T(8,128)(2,1)} %param.14) | copy-start | bytes 6488068
  113.7 2.0 copy-start
  197.9 9.9 %copy-start.1 = (f32[768,1408]{1,0:T(8,128)S(1)}, f32[768,1408]{1,0:T(8,128)}, u32[]{:S(2)}) copy-start(f32[768,1408]{1,0:T(8,128)} %copy-done) | copy-start | bytes 12976132
  207.9 4.4 copy-start.4
  210.9 1.3 copy-start.5
  227.4 235.4 %reduce-scatter.3.cloned.1.call-start = ((), (), s32[]{:S(2)}) async-start(), calls=%async_computation.5 | async-start | bytes 3932160 | tf_op jit(solution)/shard_map/reduce_scatter | solution.py:82
  235.2 46.0 %copy-start.8 = (f32[3,1408]{1,0:T(4,128)S(1)}, f32[3,1408]{1,0:T(4,128)}, u32[]{:S(2)}) copy-start(f32[3,1408]{1,0:T(4,128)} %param.17) | copy-start | bytes 50692
  281.8 9.0 %copy-start.9 = (bf16[768,2048]{1,0:T(8,128)(2,1)S(1)}, bf16[768,2048]{1,0:T(8,128)(2,1)}, u32[]{:S(2)}) copy-start(bf16[768,2048]{1,0:T(8,128)(2,1)} %all-gather.4.cloned.1.call-done) | copy-start | bytes 9437188
  310.8 113.6 %copy-start.6 = (f32[256,1408]{1,0:T(8,128)S(1)}, f32[256,1408]{1,0:T(8,128)}, u32[]{:S(2)}) copy-start(f32[256,1408]{1,0:T(8,128)} %param.16) | copy-start | bytes 4325380
  422.7 1.8 copy-start.7
Sparse Core Ops, SparseCore 0:
  10.2 95.0 all-gather.5
  107.4 90.4 all-gather.7
  199.5 26.6 all-gather.3
  229.7 193.0 reduce-scatter.4
  425.7 36.9 reduce-scatter.2
